TPU v7x, 512 devices: a 4x2x32 block of a 4x8x32 slice. The times are simulated.
512 devices in a mesh: grp: 2 (over y), fs: 32 (over z), tp: 8 (over x, core).
Axes of the slice: x: 4, y: 2, z: 32, core: 2. Of those that a mesh axis runs over, the one named last changes fastest.
The devices are a block of a 4x8x32 slice.
Arguments:
- tokens: bfloat16 [20480, 2048], P(('grp', 'fs', 'tp')), parts along dimension 0, may hold values from -6 to 6
- mix_gain: bfloat16 [2048], replicated, may hold values from 0.099609375 to 1.8984375
- val_weight: bfloat16 [2048, 1024], P('fs', 'tp'), may hold values from -4 to 4
- gate_weight: bfloat16 [2048, 1024], P('fs', 'tp'), may hold values from -0.125 to 0.125
- conv_taps: bfloat16 [31, 1024], replicated, may hold values from -1 to 1
- chan_gain: bfloat16 [1024], replicated, may hold values from 0.099609375 to 1.8984375
- out_weight: bfloat16 [1024, 2048], P('tp', 'fs'), may hold values from -0.1875 to 0.1875
- mix_post_gain: bfloat16 [2048], replicated, may hold values from 0.099609375 to 1.8984375
- ffn_gain: bfloat16 [2048], replicated, may hold values from 0.099609375 to 1.8984375
- up_gate_weight: bfloat16 [2048, 5120], P('fs', 'tp'), may hold values from -0.125 to 0.125
- up_val_weight: bfloat16 [2048, 5120], P('fs', 'tp'), may hold values from -0.125 to 0.125
- ffn_taps: bfloat16 [2, 3, 5120], replicated, may hold values from -3.5 to 3.5
- down_weight: bfloat16 [5120, 2048], P('tp', 'fs'), may hold values from -0.078125 to 0.078125
- ffn_post_gain: bfloat16 [2048], replicated, may hold values from 0.099609375 to 1.8984375
Outputs:
- layer_out: bfloat16 [20480, 2048], P(('grp', 'fs', 'tp')), parts along dimension 0
There are 2 independent parts, one for each index of `grp`. A program takes and returns all parts, laid end to end along the dimension named above; an argument that names none is the same for every part. Nothing has to cross between parts.
All inputs are finite; a program needn't handle non-finite values.
Results may differ from a plain program's by a relative error of at most 0.019.
Values may be sent and summed in bfloat16 or wider, within the bound.
A program may use at most 64 MiB of HBM per device.

v0:
```python
import jax
import jax.numpy as jnp
from jax import lax
from jax.sharding import PartitionSpec as P

LEN = 64
norm_epsilon = 1e-06
chan_epsilon = 1e-05


def from_everyone(array, axis):
    copies = jnp.broadcast_to(array, (lax.axis_size(axis), *array.shape))
    return lax.all_to_all(copies, axis, split_axis=0, concat_axis=0, tiled=True)


def laid_out(blocks, dim):
    blocks = jnp.moveaxis(blocks, 0, dim)
    lengths = blocks.shape
    return blocks.reshape(*lengths[:dim], lengths[dim] * lengths[dim + 1], *lengths[dim + 2 :])


def gathered_copies(array, axis, dim):
    blocks = from_everyone(array, axis)
    return laid_out(blocks, dim)


def sent_together(arrays, axis, dim, along):
    ends, at = ([], 0)
    for a in arrays[:-1]:
        at += a.shape[along]
        ends.append(at)
    both = jnp.concatenate(arrays, axis=along)
    return tuple(jnp.split(lax.all_gather(both, axis, axis=dim, tiled=True), ends, axis=along))


def over_copies(array, axis):
    return from_everyone(array, axis).sum(axis=0)


def together(arrays, axis):
    ends = [0]
    for a in arrays:
        ends.append(ends[-1] + a.size)
    total = over_copies(jnp.concatenate([a.ravel() for a in arrays]), axis)
    return tuple((total[b:e].reshape(a.shape) for a, b, e in zip(arrays, ends, ends[1:])))


def in_blocks(array, dim, length):
    lengths = array.shape
    blocks = array.reshape(*lengths[:dim], length, lengths[dim] // length, *lengths[dim + 1 :])
    return jnp.moveaxis(blocks, dim, 0)


def summed_on_arrival(array, axis, dim):
    blocks = in_blocks(array, dim, lax.axis_size(axis))
    arrived = lax.all_to_all(blocks, axis, split_axis=0, concat_axis=0, tiled=True)
    return arrived.astype(jnp.float32).sum(axis=0)


def rms_scale(values, gain):
    inverse = lax.rsqrt(jnp.mean(values * values, axis=-1, keepdims=True) + norm_epsilon)
    return values * inverse * gain.astype(jnp.float32)


def depthwise(signal, tap_table):
    taps_count = tap_table.shape[0]
    channels = signal.shape[1]
    shaped = signal.astype(jnp.float32).reshape(signal.shape[0] // LEN, LEN, channels)
    padded = jnp.pad(shaped, ((0, 0), (taps_count - 1, 0), (0, 0)))
    tap_values = tap_table.astype(jnp.float32)
    result = jnp.zeros(shaped.shape, jnp.float32)
    for offset in range(taps_count):
        result = result + padded[:, offset : offset + LEN, :] * tap_values[offset]
    return result.reshape(signal.shape[0], channels)


def make_adder(left, pieces):
    first = jnp.dot(left, pieces[0], preferred_element_type=jnp.float32)
    second = jnp.dot(left, pieces[1], preferred_element_type=jnp.float32)
    return (first, second)


def make_rows_product(left, weight):
    return jnp.dot(left, weight, preferred_element_type=jnp.float32)


def shards(
    tokens,
    mix_gain,
    val_weight,
    gate_weight,
    conv_taps,
    chan_gain,
    out_weight,
    mix_post_gain,
    ffn_gain,
    up_gate_weight,
    up_val_weight,
    ffn_taps,
    down_weight,
    ffn_post_gain,
):
    member = lax.axis_index("tp")
    normed_own = rms_scale(tokens.astype(jnp.float32), mix_gain).astype(jnp.bfloat16)
    normed = gathered_copies(normed_own, "tp", 0)
    local_ch = val_weight.shape[1]
    values, gate_sums = make_adder(normed, sent_together((val_weight, gate_weight), "fs", 0, 1))
    glu_out = (values * jax.nn.sigmoid(gate_sums)).astype(jnp.bfloat16)
    own_taps = lax.dynamic_slice_in_dim(conv_taps, member * local_ch, local_ch, 1)
    conv_out = depthwise(glu_out, own_taps)
    totals, squares = together(
        (jnp.sum(conv_out, axis=1), jnp.sum(conv_out * conv_out, axis=1)), "tp"
    )
    all_channels = chan_gain.shape[0]
    chan_mean = totals[:, None] / all_channels
    chan_var = squares[:, None] / all_channels - chan_mean * chan_mean
    own_gain = lax.dynamic_slice_in_dim(chan_gain, member * local_ch, local_ch, 0).astype(
        jnp.float32
    )
    activated = jax.nn.silu((conv_out - chan_mean) * lax.rsqrt(chan_var + chan_epsilon) * own_gain)
    activated = activated.astype(jnp.bfloat16)
    out_full = lax.all_gather(out_weight, "fs", axis=1, tiled=True)
    mixed_sum = summed_on_arrival(
        make_rows_product(activated, out_full).astype(jnp.bfloat16), "tp", 0
    )
    residual = (tokens.astype(jnp.float32) + rms_scale(mixed_sum, mix_post_gain)).astype(
        jnp.bfloat16
    )
    normed_share = rms_scale(residual.astype(jnp.float32), ffn_gain).astype(jnp.bfloat16)
    normed_ffn = gathered_copies(normed_share, "tp", 0)
    local_ff = up_gate_weight.shape[1]
    own_ffn_taps = lax.dynamic_slice_in_dim(ffn_taps, member * local_ff, local_ff, 2)
    gate_full, val_full = sent_together((up_gate_weight, up_val_weight), "fs", 0, 1)
    up_gate = jnp.dot(normed_ffn, gate_full, preferred_element_type=jnp.float32).astype(
        jnp.bfloat16
    )
    up_val = jnp.dot(normed_ffn, val_full, preferred_element_type=jnp.float32).astype(jnp.bfloat16)
    gate_conv = depthwise(up_gate, own_ffn_taps[0])
    val_conv = depthwise(up_val, own_ffn_taps[1])
    hidden = (jax.nn.gelu(gate_conv, approximate=True) * val_conv).astype(jnp.bfloat16)
    down_full = lax.all_gather(down_weight, "fs", axis=1, tiled=True)
    ffn_sum = summed_on_arrival(make_rows_product(hidden, down_full).astype(jnp.bfloat16), "tp", 0)
    return (residual.astype(jnp.float32) + rms_scale(ffn_sum, ffn_post_gain)).astype(jnp.bfloat16)


def solution(mesh):
    return jax.shard_map(
        shards,
        mesh=mesh,
        in_specs=(
            P(("grp", "fs", "tp"), None),
            P(),
            P("fs", "tp"),
            P("fs", "tp"),
            P(),
            P(),
            P("tp", "fs"),
            P(),
            P(),
            P("fs", "tp"),
            P("fs", "tp"),
            P(),
            P("tp", "fs"),
            P(),
        ),
        out_specs=P(("grp", "fs", "tp"), None),
        check_vma=False,
    )
```

profile of v0, /device:TPU:33, one launch (start us, length us, event | category | flops | bytes accessed | tf_op | source)
XLA Modules:
  0.0 472.4 jit_solution(905065115232511449)
XLA Ops:
  6.6 1.3 pad_maximum_fusion.1
  8.0 1.6 pad_maximum_fusion
  9.7 0.7 convert_element_type.82
  10.4 1.1 fusion.33
  11.5 1.0 fusion.35
  12.5 1.3 broadcast_in_dim.6
  13.7 45.0 %all-to-all-start = ((bf16[8,40,2048]{2,1,0:T(8,128)(2,1)}), bf16[8,40,2048]{2,1,0:T(8,128)(2,1)S(1)}, u32[]{:S(2)}, u32[]{:S(2)}) async-start(bf16[8,40,2048]{2,1,0:T(8,128)(2,1)} %broadcast_in_dim.6), calls=%async_computation | async-start | bytes 2621440 | tf_op jit(solution)/shard_map/all_to_all | solution.py:13
  58.8 0.7 dynamic-slice_convert_fusion
  59.5 46.8 %all_gather.13 = bf16[128,2048]{0,1:T(8,128)(2,1)S(1)} all-gather(bf16[128,64]{0,1:T(8,128)(2,1)S(1)} %copy-done.2), channel_id=1, replica_groups=mesh['grp'=2,'fs'=32,'tp'=8] {'fs'}, dimensions={1}, use_global_device_ids=true | all-gather | bytes 540672 | tf_op jit(solution)/shard_map/all_gather | solution.py:122
  106.3 43.0 %all-gather.4.cloned.1.call-done = bf16[2048,256]{1,0:T(8,128)(2,1)} async-done(((bf16[64,256]{1,0:T(8,128)(2,1)}), bf16[2048,256]{1,0:T(8,128)(2,1)}) %all-gather.4.cloned.1.call-update) | async-done | bytes 1048592 | tf_op jit(solution)/shard_map/all_gather | solution.py:33
  149.3 1.6 fusion.12
  151.5 0.6 fusion.103
  152.4 0.6 broadcast_in_dim.7
  153.0 25.4 %all-to-all-start.1 = ((f32[8,1,640]{2,1,0:T(1,128)}), f32[8,1,640]{2,1,0:T(1,128)S(1)}, u32[]{:S(2)}, u32[]{:S(2)}) async-start(f32[8,1,640]{2,1,0:T(1,128)} %broadcast_in_dim.7), calls=%async_computation.1 | async-start | bytes 40960 | tf_op jit(solution)/shard_map/all_to_all | solution.py:13
  178.4 0.8 dynamic-slice_convert_fusion.3
  179.2 3.9 all-to-all-done.1
  183.4 1.7 convolution_convert_fusion
  185.1 4.3 all-to-all-start.2
  189.4 0.7 all-gather.8.cloned.1.call-update
  190.2 17.1 %all-to-all-done.2 = bf16[8,40,2048]{2,1,0:T(8,128)(2,1)S(1)} async-done(((bf16[8,40,2048]{2,1,0:T(8,128)(2,1)}), bf16[8,40,2048]{2,1,0:T(8,128)(2,1)S(1)}, u32[]{:S(2)}, u32[]{:S(2)}) %all-to-all-start.2) | async-done | bytes 1310752 | tf_op jit(solution)/shard_map/all_to_all | solution.py:56
  208.0 1.3 broadcast_in_dim.8
  209.3 4.4 all-to-all-start.3
  213.8 0.9 dynamic-slice_convert_fusion.2
  214.7 17.0 %all-to-all-done.3 = bf16[8,40,2048]{2,1,0:T(8,128)(2,1)S(1)} async-done(((bf16[8,40,2048]{2,1,0:T(8,128)(2,1)}), bf16[8,40,2048]{2,1,0:T(8,128)(2,1)S(1)}, u32[]{:S(2)}, u32[]{:S(2)}) %all-to-all-start.3) | async-done | bytes 1310752 | tf_op jit(solution)/shard_map/all_to_all | solution.py:13
  231.6 55.6 %all-gather.6.cloned.1.call-done = bf16[2048,1280]{1,0:T(8,128)(2,1)} async-done(((bf16[64,1280]{1,0:T(8,128)(2,1)}), bf16[2048,1280]{1,0:T(8,128)(2,1)}) %all-gather.6.cloned.1.call-update) | async-done | bytes 5242896 | tf_op jit(solution)/shard_map/all_gather | solution.py:33
  287.2 3.1 fusion.4
  290.5 1.2 fusion.7
  292.5 124.9 %all-gather.8.cloned.1.call-done = bf16[640,2048]{0,1:T(8,128)(2,1)} async-done(((bf16[640,64]{0,1:T(8,128)(2,1)}), bf16[640,2048]{0,1:T(8,128)(2,1)}) %all-gather.8.cloned.1.call-update) | async-done | bytes 2621456 | tf_op jit(solution)/shard_map/all_gather | solution.py:141
  417.5 4.0 convolution_convert_fusion.1
  421.5 25.5 %all-to-all-start.4 = ((bf16[8,40,2048]{2,1,0:T(8,128)(2,1)}), bf16[8,40,2048]{2,1,0:T(8,128)(2,1)S(1)}, u32[]{:S(2)}, u32[]{:S(2)}) async-start(bf16[8,40,2048]{2,1,0:T(8,128)(2,1)} %bitcast.43), calls=%async_computation.4 | async-start | bytes 2621440 | tf_op jit(solution)/shard_map/all_to_all | solution.py:56
  447.0 17.8 %all-to-all-done.4 = bf16[8,40,2048]{2,1,0:T(8,128)(2,1)S(1)} async-done(((bf16[8,40,2048]{2,1,0:T(8,128)(2,1)}), bf16[8,40,2048]{2,1,0:T(8,128)(2,1)S(1)}, u32[]{:S(2)}, u32[]{:S(2)}) %all-to-all-start.4) | async-done | bytes 1310752 | tf_op jit(solution)/shard_map/all_to_all | solution.py:56
  465.1 0.8 fusion.40
  (49 shorter events, 3.4 us)
Async XLA Ops:
  6.5 142.8 %all-gather.4.cloned.1.call-start = ((), (), s32[]{:S(2)}) async-start(), calls=%async_computation.5 | async-start | bytes 1081344 | tf_op jit(solution)/shard_map/all_gather | solution.py:33
  8.0 279.3 %all-gather.6.cloned.1.call-start = ((), (), s32[]{:S(2)}) async-start(), calls=%async_computation.6 | async-start | bytes 5406720 | tf_op jit(solution)/shard_map/all_gather | solution.py:33
  13.7 45.8 %copy-start.2 = (bf16[128,64]{0,1:T(8,128)(2,1)S(1)}, bf16[128,64]{0,1:T(8,128)(2,1)}, u32[]{:S(2)}) copy-start(bf16[128,64]{0,1:T(8,128)(2,1)} %param.20) | copy-start | bytes 49156
  13.7 92.6 %all-to-all-start = ((bf16[8,40,2048]{2,1,0:T(8,128)(2,1)}), bf16[8,40,2048]{2,1,0:T(8,128)(2,1)S(1)}, u32[]{:S(2)}, u32[]{:S(2)}) async-start(bf16[8,40,2048]{2,1,0:T(8,128)(2,1)} %broadcast_in_dim.6), calls=%async_computation | async-start | bytes 2621440 | tf_op jit(solution)/shard_map/all_to_all | solution.py:13
  149.3 1.7 copy-start.1
  153.0 30.1 %all-to-all-start.1 = ((f32[8,1,640]{2,1,0:T(1,128)}), f32[8,1,640]{2,1,0:T(1,128)S(1)}, u32[]{:S(2)}, u32[]{:S(2)}) async-start(f32[8,1,640]{2,1,0:T(1,128)} %broadcast_in_dim.7), calls=%async_computation.1 | async-start | bytes 40960 | tf_op jit(solution)/shard_map/all_to_all | solution.py:13
  185.1 5.1 %copy-start.3 = (bf16[2048]{0:T(1024)(128)(2,1)S(1)}, bf16[2048]{0:T(1024)(128)(2,1)}, u32[]{:S(2)}) copy-start(bf16[2048]{0:T(1024)(128)(2,1)} %param.21) | copy-start | bytes 12292
  185.1 5.1 %copy-start.4 = (bf16[2048]{0:T(1024)(128)(2,1)S(1)}, bf16[2048]{0:T(1024)(128)(2,1)}, u32[]{:S(2)}) copy-start(bf16[2048]{0:T(1024)(128)(2,1)} %param.22) | copy-start | bytes 12292
  185.1 22.2 %all-to-all-start.2 = ((bf16[8,40,2048]{2,1,0:T(8,128)(2,1)}), bf16[8,40,2048]{2,1,0:T(8,128)(2,1)S(1)}, u32[]{:S(2)}, u32[]{:S(2)}) async-start(bf16[8,40,2048]{2,1,0:T(8,128)(2,1)} %bitcast.35), calls=%async_computation.2 | async-start | bytes 2621440 | tf_op jit(solution)/shard_map/all_to_all | solution.py:56
  189.4 18.2 %copy-start = (bf16[40,2048]{1,0:T(8,128)(2,1)S(1)}, bf16[40,2048]{1,0:T(8,128)(2,1)}, u32[]{:S(2)}) copy-start(bf16[40,2048]{1,0:T(8,128)(2,1)} %param.14) | copy-start | bytes 491524
  189.4 228.1 %all-gather.8.cloned.1.call-start = ((), (), s32[]{:S(2)}) async-start(), calls=%async_computation.7 | async-start | bytes 2703360 | tf_op jit(solution)/shard_map/all_gather | solution.py:141
  209.3 22.3 %all-to-all-start.3 = ((bf16[8,40,2048]{2,1,0:T(8,128)(2,1)}), bf16[8,40,2048]{2,1,0:T(8,128)(2,1)S(1)}, u32[]{:S(2)}, u32[]{:S(2)}) async-start(bf16[8,40,2048]{2,1,0:T(8,128)(2,1)} %broadcast_in_dim.8), calls=%async_computation.3 | async-start | bytes 2621440 | tf_op jit(solution)/shard_map/all_to_all | solution.py:13
  287.2 3.3 copy-start.6
  421.5 25.5 %copy-start.5 = (bf16[2048]{0:T(1024)(128)(2,1)S(1)}, bf16[2048]{0:T(1024)(128)(2,1)}, u32[]{:S(2)}) copy-start(bf16[2048]{0:T(1024)(128)(2,1)} %param.27) | copy-start | bytes 12292
  421.5 43.3 %all-to-all-start.4 = ((bf16[8,40,2048]{2,1,0:T(8,128)(2,1)}), bf16[8,40,2048]{2,1,0:T(8,128)(2,1)S(1)}, u32[]{:S(2)}, u32[]{:S(2)}) async-start(bf16[8,40,2048]{2,1,0:T(8,128)(2,1)} %bitcast.43), calls=%async_computation.4 | async-start | bytes 2621440 | tf_op jit(solution)/shard_map/all_to_all | solution.py:56
Sparse Core Ops, SparseCore 0:
  9.4 139.8 all-gather.3
  151.4 135.7 all-gather.5
  289.3 128.1 all-gather.7
where the time goes:
time: 473 us; the launch traced here: 472 us
  waiting for transfers between devices  280 us (59%)
  starting transfers between devices  105 us (22%)
  blocking collectives  46.8 us (10%)
  between operations  13.3 us (3%)
  matrix products  12.1 us (3%)
  other arithmetic  11.8 us (2%)
    all_gather x1, waiting for transfers between devices, shards(): down_full = lax.all_gather(down_weight, 'fs', axis=1, tiled=True)  125 us
    all_gather x2, waiting for transfers between devices, sent_together(): lax.all_gather(both, axis, axis=dim, tiled=True)  98.6 us
    all_to_all x3, starting transfers between devices, from_everyone(): return lax.all_to_all(copies, axis, split_axis=0, concat_axis=0, tiled=True)  74.9 us
    all_gather x1, blocking collectives, shards(): out_full = lax.all_gather(out_weight, 'fs', axis=1, tiled=True)  46.8 us
    all_to_all x2, waiting for transfers between devices, summed_on_arrival(): lax.all_to_all(blocks, axis, split_axis=0, concat_axis=0, tiled=True)  34.8 us
    all_to_all x2, starting transfers between devices, summed_on_arrival(): lax.all_to_all(blocks, axis, split_axis=0, concat_axis=0, tiled=True)  29.8 us
    all_to_all x3, waiting for transfers between devices, from_everyone(): return lax.all_to_all(copies, axis, split_axis=0, concat_axis=0, tiled=True)  20.9 us
  transfers between devices with their start and end apart: 8, of which 7 were waited for; matrix products, arithmetic and copies ran while one was open for 4% of the time, Pallas kernels for 0%

commit v1 on v0

--- a/solution.py
+++ b/solution.py
@@ -2,6 +2,7 @@
 import jax.numpy as jnp
 from jax import lax
 from jax.sharding import PartitionSpec as P
+from jax.lax import all_to_all, axis_size
 
 LEN = 64
 norm_epsilon = 1e-06
@@ -138,7 +139,9 @@
     gate_conv = depthwise(up_gate, own_ffn_taps[0])
     val_conv = depthwise(up_val, own_ffn_taps[1])
     hidden = (jax.nn.gelu(gate_conv, approximate=True) * val_conv).astype(jnp.bfloat16)
-    down_full = lax.all_gather(down_weight, "fs", axis=1, tiled=True)
+    base_arr = jnp.stack([down_weight for _ in range(axis_size("fs"))])
+    n_now = all_to_all(base_arr, "fs", 0, 0)
+    down_full = jnp.concatenate(n_now, axis=1)
     ffn_sum = summed_on_arrival(make_rows_product(hidden, down_full).astype(jnp.bfloat16), "tp", 0)
     return (residual.astype(jnp.float32) + rms_scale(ffn_sum, ffn_post_gain)).astype(jnp.bfloat16)
 

time: 473 us -> 603 us (1.27)
  waiting for transfers between devices: 280 us -> 389 us
  blocking collectives: 46.8 us -> 69.8 us
    all_gather x2, waiting for transfers between devices: 98.6 us -> 349 us  [sent_together(): lax.all_gather(both, axis, axis=dim, tiled=True)]
    all_gather x1 -> x0, waiting for transfers between devices: 125 us -> none  [shards(): down_full = lax.all_gather(down_weight, 'fs', axis=1, tiled=True)]
    all_to_all x0 -> x1, blocking collectives: none -> 22 us  [from_everyone(): return lax.all_to_all(copies, axis, split_axis=0, concat_axis=0, tiled=True)]
    all_to_all x3 -> x2, waiting for transfers between devices: 20.9 us -> 3.92 us  [from_everyone(): return lax.all_to_all(copies, axis, split_axis=0, concat_axis=0, tiled=True)]
    all_to_all x0 -> x1, starting transfers between devices: none -> 13 us  [shards(): n_now = all_to_all(base_arr, 'fs', 0, 0)]
    all_to_all x2, starting transfers between devices: 29.8 us -> 19.6 us  [summed_on_arrival(): lax.all_to_all(blocks, axis, split_axis=0, concat_axis=0, tiled=True)]
    all_to_all x3 -> x2, starting transfers between devices: 74.9 us -> 71.1 us  [from_everyone(): return lax.all_to_all(copies, axis, split_axis=0, concat_axis=0, tiled=True)]
  transfers between devices with their start and end apart: 8 -> 7, of which waited for: 7 -> 5; matrix products, arithmetic and copies ran while one was open for 4% -> 2% of each run, Pallas kernels for 0% -> 0%
where the time goes in v1:
time: 603 us; the launch traced here: 602 us
  waiting for transfers between devices  389 us (65%)
  starting transfers between devices  104 us (17%)
  blocking collectives  69.8 us (12%)
  between operations  13.7 us (2%)
  other arithmetic  10.9 us (2%)
  matrix products  10.7 us (2%)
    all_gather x2, waiting for transfers between devices, sent_together(): lax.all_gather(both, axis, axis=dim, tiled=True)  349 us
    all_to_all x2, starting transfers between devices, from_everyone(): return lax.all_to_all(copies, axis, split_axis=0, concat_axis=0, tiled=True)  71.1 us
    all_gather x1, blocking collectives, shards(): out_full = lax.all_gather(out_weight, 'fs', axis=1, tiled=True)  47.8 us
    all_to_all x2, waiting for transfers between devices, summed_on_arrival(): lax.all_to_all(blocks, axis, split_axis=0, concat_axis=0, tiled=True)  35.7 us
    all_to_all x1, blocking collectives, from_everyone(): return lax.all_to_all(copies, axis, split_axis=0, concat_axis=0, tiled=True)  22 us
    all_to_all x2, starting transfers between devices, summed_on_arrival(): lax.all_to_all(blocks, axis, split_axis=0, concat_axis=0, tiled=True)  19.6 us
    all_to_all x1, starting transfers between devices, shards(): n_now = all_to_all(base_arr, 'fs', 0, 0)  13 us
  transfers between devices with their start and end apart: 7, of which 5 were waited for; matrix products, arithmetic and copies ran while one was open for 2% of the time, Pallas kernels for 0%

profile of v1, /device:TPU:33, one launch (start us, length us, event | category | flops | bytes accessed | tf_op | source)
XLA Modules:
  0.0 602.3 jit_solution(16608837954158282103)
XLA Ops:
  6.6 1.4 pad_maximum_fusion.1
  8.0 0.7 convert_element_type.85
  8.7 1.1 fusion.33
  9.7 1.0 fusion.35
  10.8 1.2 broadcast_in_dim.6
  12.0 45.0 %all-to-all-start = ((bf16[8,40,2048]{2,1,0:T(8,128)(2,1)}), bf16[8,40,2048]{2,1,0:T(8,128)(2,1)S(1)}, u32[]{:S(2)}, u32[]{:S(2)}) async-start(bf16[8,40,2048]{2,1,0:T(8,128)(2,1)} %broadcast_in_dim.6), calls=%async_computation | async-start | bytes 2621440 | tf_op jit(solution)/shard_map/all_to_all | solution.py:14
  57.0 0.7 dynamic-slice_convert_fusion
  57.8 47.8 %all_gather.10 = bf16[128,2048]{0,1:T(8,128)(2,1)S(1)} all-gather(bf16[128,64]{0,1:T(8,128)(2,1)S(1)} %copy-done.6), channel_id=1, replica_groups=mesh['grp'=2,'fs'=32,'tp'=8] {'fs'}, dimensions={1}, use_global_device_ids=true | all-gather | bytes 540672 | tf_op jit(solution)/shard_map/all_gather | solution.py:123
  105.5 43.3 %all-gather.3.cloned.1.call-done = bf16[2048,256]{1,0:T(8,128)(2,1)} async-done(((bf16[64,256]{1,0:T(8,128)(2,1)}), bf16[2048,256]{1,0:T(8,128)(2,1)}) %all-gather.3.cloned.1.call-update) | async-done | bytes 1048592 | tf_op jit(solution)/shard_map/all_gather | solution.py:34
  148.8 1.6 fusion.12
  151.0 0.6 fusion.103
  151.9 0.6 broadcast_in_dim.7
  152.5 26.1 %all-to-all-start.1 = ((f32[8,1,640]{2,1,0:T(1,128)}), f32[8,1,640]{2,1,0:T(1,128)S(1)}, u32[]{:S(2)}, u32[]{:S(2)}) async-start(f32[8,1,640]{2,1,0:T(1,128)} %broadcast_in_dim.7), calls=%async_computation.1 | async-start | bytes 40960 | tf_op jit(solution)/shard_map/all_to_all | solution.py:14
  178.6 0.8 dynamic-slice_convert_fusion.3
  179.3 3.9 all-to-all-done.1
  183.5 1.6 convolution_convert_fusion
  185.1 4.3 all-to-all-start.2
  189.5 17.8 %all-to-all-done.2 = bf16[8,40,2048]{2,1,0:T(8,128)(2,1)S(1)} async-done(((bf16[8,40,2048]{2,1,0:T(8,128)(2,1)}), bf16[8,40,2048]{2,1,0:T(8,128)(2,1)S(1)}, u32[]{:S(2)}, u32[]{:S(2)}) %all-to-all-start.2) | async-done | bytes 1310752 | tf_op jit(solution)/shard_map/all_to_all | solution.py:57
  208.2 22.0 %all_to_all.31 = bf16[8,40,2048]{2,1,0:T(8,128)(2,1)} all-to-all(bf16[8,40,2048]{2,1,0:T(8,128)(2,1)S(1)} %broadcast_in_dim.8), channel_id=1, replica_groups=mesh['grp'=2,'fs'=32,'tp'=8] {'tp'}, dimensions={0} | all-to-all | bytes 2621440 | tf_op jit(solution)/shard_map/all_to_all | solution.py:14
  230.2 1.9 stack.2
  232.1 13.0 %all-to-all-start.4 = ((bf16[32,640,64]{1,2,0:T(8,128)(2,1)}), bf16[32,640,64]{1,2,0:T(8,128)(2,1)S(1)}, u32[]{:S(2)}, u32[]{:S(2)}) async-start(bf16[32,640,64]{1,2,0:T(8,128)(2,1)} %stack.2), calls=%async_computation.4 | async-start | bytes 5242880 | tf_op jit(solution)/shard_map/all_to_all | solution.py:143
  245.2 0.7 pad_maximum_fusion
  245.9 0.9 dynamic-slice_convert_fusion.2
  246.9 305.9 %all-gather.5.cloned.1.call-done = bf16[2048,1280]{1,0:T(8,128)(2,1)} async-done(((bf16[64,1280]{1,0:T(8,128)(2,1)}), bf16[2048,1280]{1,0:T(8,128)(2,1)}) %all-gather.5.cloned.1.call-update) | async-done | bytes 5242896 | tf_op jit(solution)/shard_map/all_gather | solution.py:34
  552.7 3.5 fusion.4
  556.3 0.5 copy-done.10
  556.8 1.2 fusion.7
  558.1 0.8 fusion.22
  558.9 2.3 convolution_convert_fusion.1
  561.2 15.3 %all-to-all-start.5 = ((bf16[8,40,2048]{2,1,0:T(8,128)(2,1)}), bf16[8,40,2048]{2,1,0:T(8,128)(2,1)S(1)}, u32[]{:S(2)}, u32[]{:S(2)}) async-start(bf16[8,40,2048]{2,1,0:T(8,128)(2,1)} %bitcast.97), calls=%async_computation.5 | async-start | bytes 2621440 | tf_op jit(solution)/shard_map/all_to_all | solution.py:57
  576.5 17.9 %all-to-all-done.5 = bf16[8,40,2048]{2,1,0:T(8,128)(2,1)S(1)} async-done(((bf16[8,40,2048]{2,1,0:T(8,128)(2,1)}), bf16[8,40,2048]{2,1,0:T(8,128)(2,1)S(1)}, u32[]{:S(2)}, u32[]{:S(2)}) %all-to-all-start.5) | async-done | bytes 1310752 | tf_op jit(solution)/shard_map/all_to_all | solution.py:57
  594.7 0.8 fusion.40
  (54 shorter events, 2.6 us)
Async XLA Ops:
  6.5 142.3 %all-gather.3.cloned.1.call-start = ((), (), s32[]{:S(2)}) async-start(), calls=%async_computation.6 | async-start | bytes 1081344 | tf_op jit(solution)/shard_map/all_gather | solution.py:34
  12.0 45.8 %copy-start.6 = (bf16[128,64]{0,1:T(8,128)(2,1)S(1)}, bf16[128,64]{0,1:T(8,128)(2,1)}, u32[]{:S(2)}) copy-start(bf16[128,64]{0,1:T(8,128)(2,1)} %param.20) | copy-start | bytes 49156
  12.0 93.5 %all-to-all-start = ((bf16[8,40,2048]{2,1,0:T(8,128)(2,1)}), bf16[8,40,2048]{2,1,0:T(8,128)(2,1)S(1)}, u32[]{:S(2)}, u32[]{:S(2)}) async-start(bf16[8,40,2048]{2,1,0:T(8,128)(2,1)} %broadcast_in_dim.6), calls=%async_computation | async-start | bytes 2621440 | tf_op jit(solution)/shard_map/all_to_all | solution.py:14
  148.8 1.7 copy-start.2
  152.5 30.7 %all-to-all-start.1 = ((f32[8,1,640]{2,1,0:T(1,128)}), f32[8,1,640]{2,1,0:T(1,128)S(1)}, u32[]{:S(2)}, u32[]{:S(2)}) async-start(f32[8,1,640]{2,1,0:T(1,128)} %broadcast_in_dim.7), calls=%async_computation.1 | async-start | bytes 40960 | tf_op jit(solution)/shard_map/all_to_all | solution.py:14
  185.1 4.3 copy-start.7
  185.1 4.3 copy-start.8
  185.1 22.2 %all-to-all-start.2 = ((bf16[8,40,2048]{2,1,0:T(8,128)(2,1)}), bf16[8,40,2048]{2,1,0:T(8,128)(2,1)S(1)}, u32[]{:S(2)}, u32[]{:S(2)}) async-start(bf16[8,40,2048]{2,1,0:T(8,128)(2,1)} %bitcast.35), calls=%async_computation.2 | async-start | bytes 2621440 | tf_op jit(solution)/shard_map/all_to_all | solution.py:57
  189.4 18.2 %copy-start = (bf16[40,2048]{1,0:T(8,128)(2,1)S(1)}, bf16[40,2048]{1,0:T(8,128)(2,1)}, u32[]{:S(2)}) copy-start(bf16[40,2048]{1,0:T(8,128)(2,1)} %param.14) | copy-start | bytes 491524
  208.2 22.0 %copy-start.5 = (bf16[640,64]{0,1:T(8,128)(2,1)S(1)}, bf16[640,64]{0,1:T(8,128)(2,1)}, u32[]{:S(2)}) copy-start(bf16[640,64]{0,1:T(8,128)(2,1)} %param.26) | copy-start | bytes 245764
  232.1 13.1 %copy-start.3 = (bf16[64,640]{1,0:T(8,128)(2,1)S(1)}, bf16[64,640]{1,0:T(8,128)(2,1)}, u32[]{:S(2)}) copy-start(bf16[64,640]{1,0:T(8,128)(2,1)} %param.24) | copy-start | bytes 245764
  232.1 13.1 %copy-start.4 = (bf16[64,640]{1,0:T(8,128)(2,1)S(1)}, bf16[64,640]{1,0:T(8,128)(2,1)}, u32[]{:S(2)}) copy-start(bf16[64,640]{1,0:T(8,128)(2,1)} %param.23) | copy-start | bytes 245764
  232.1 326.8 %all-to-all-start.4 = ((bf16[32,640,64]{1,2,0:T(8,128)(2,1)}), bf16[32,640,64]{1,2,0:T(8,128)(2,1)S(1)}, u32[]{:S(2)}, u32[]{:S(2)}) async-start(bf16[32,640,64]{1,2,0:T(8,128)(2,1)} %stack.2), calls=%async_computation.4 | async-start | bytes 5242880 | tf_op jit(solution)/shard_map/all_to_all | solution.py:143
  245.1 307.6 %all-gather.5.cloned.1.call-start = ((), (), s32[]{:S(2)}) async-start(), calls=%async_computation.7 | async-start | bytes 5406720 | tf_op jit(solution)/shard_map/all_gather | solution.py:34
  552.7 3.5 copy-start.1
  552.7 4.1 copy-start.10
  561.2 15.3 %copy-start.9 = (bf16[2048]{0:T(1024)(128)(2,1)S(1)}, bf16[2048]{0:T(1024)(128)(2,1)}, u32[]{:S(2)}) copy-start(bf16[2048]{0:T(1024)(128)(2,1)} %param.27) | copy-start | bytes 12292
  561.2 33.2 %all-to-all-start.5 = ((bf16[8,40,2048]{2,1,0:T(8,128)(2,1)}), bf16[8,40,2048]{2,1,0:T(8,128)(2,1)S(1)}, u32[]{:S(2)}, u32[]{:S(2)}) async-start(bf16[8,40,2048]{2,1,0:T(8,128)(2,1)} %bitcast.97), calls=%async_computation.5 | async-start | bytes 2621440 | tf_op jit(solution)/shard_map/all_to_all | solution.py:57
Sparse Core Ops, SparseCore 0:
  9.4 139.3 all-gather.2
  248.0 304.6 all-gather.4
